TPU v7x, 32 devices: a whole 2x2x4 slice. The times are simulated.
32 devices in a mesh: fs: 16 (over z, y, x), tp: 2 (over core).
Axes of the slice: x: 2, y: 2, z: 4, core: 2. Of those that a mesh axis runs over, the one named last changes fastest.
Arguments:
- tokens: bfloat16 [6144, 2048], P('fs', 'tp'), may hold values from -24 to 24
- mixer_gain: float32 [2048], replicated, may hold values from 0.1 to 1.9
- pool_input: bfloat16 [2048, 1024], P('fs', 'tp'), may hold values from -0.125 to 0.125
- group_weight: bfloat16 [8, 128, 128], P('tp'), may hold values from -0.5 to 0.5
- channel_scale: float32 [1024], P('tp'), may hold values from 0.5 to 2
- pool_output: bfloat16 [1024, 2048], P('tp', 'fs'), may hold values from -0.1875 to 0.1875
- ffn_gain: float32 [2048], replicated, may hold values from 0.1 to 1.9
- gate_weight: bfloat16 [2048, 5632], P('fs', 'tp'), may hold values from -0.125 to 0.125
- up_weight: bfloat16 [2048, 5632], P('fs', 'tp'), may hold values from -0.125 to 0.125
- down_weight: bfloat16 [5632, 2048], P('tp', 'fs'), may hold values from -0.078125 to 0.078125
- final_gain: float32 [2048], P('tp'), may hold values from 0.1 to 1.9
Outputs:
- normed_out: bfloat16 [6144, 2048], P('fs', 'tp')
All inputs are finite; a program needn't handle non-finite values.
Results may differ from a plain program's by a relative error of at most 0.015.
Values may be sent and summed in bfloat16 or wider, within the bound.
No kernel may reach another device: no remote copies, remote signals or barrier semaphores. Data moves between devices by JAX's collectives and lax.ppermute only.
A program may use at most 128 MiB of HBM per device.

v0:
```python
import jax
import jax.numpy as jnp
from jax import lax
from jax.sharding import PartitionSpec as P

D = 2048
GROUP_DIM = 128
LENGTH = 128
EPS = 1e-06


def rms(values, gain):
    wide = values.astype(jnp.float32)
    scaled = wide * lax.rsqrt(jnp.mean(wide * wide, axis=-1, keepdims=True) + EPS)
    return scaled * gain


def add_rows(left, piece):
    return jnp.dot(left, piece, preferred_element_type=jnp.float32)


def local(
    tokens,
    mixer_gain,
    pool_input,
    group_weight,
    channel_scale,
    pool_output,
    ffn_gain,
    gate_weight,
    up_weight,
    down_weight,
    final_gain,
):
    full_rows = lax.all_gather(tokens, "tp", axis=1, tiled=True)
    first_normed = rms(full_rows, mixer_gain).astype(jnp.bfloat16)
    row_count = first_normed.shape[0]
    pooled_in = add_rows(first_normed, lax.all_gather(pool_input, "fs", axis=0, tiled=True)).astype(
        jnp.bfloat16
    )
    local_groups = group_weight.shape[0]
    group_ids = lax.axis_index("tp") * local_groups + jnp.arange(local_groups, dtype=jnp.int32)
    windows = jnp.left_shift(jnp.int32(2), group_ids % 4)
    later = jnp.arange(LENGTH, dtype=jnp.int32)[None, :, None]
    earlier = jnp.arange(LENGTH, dtype=jnp.int32)[None, None, :]
    reach = windows[:, None, None]
    inside = (earlier <= later) & (earlier > later - reach)
    band = inside.astype(jnp.bfloat16)
    divisor = jnp.minimum(later[:, :, 0] + 1, windows[:, None]).astype(jnp.float32)
    grid_low = pooled_in.reshape(row_count // LENGTH, LENGTH, local_groups, GROUP_DIM)
    window_sums = jnp.einsum("gts,nsgc->ntgc", band, grid_low, preferred_element_type=jnp.float32)
    average = window_sums / jnp.transpose(divisor)[None, :, :, None]
    pooled = (
        (average - grid_low.astype(jnp.float32))
        .astype(jnp.bfloat16)
        .reshape(row_count, local_groups, GROUP_DIM)
    )
    mapped = jnp.einsum("ngc,gcd->ngd", pooled, group_weight, preferred_element_type=jnp.float32)
    grouped = (mapped.reshape(row_count, local_groups * GROUP_DIM) * channel_scale).astype(
        jnp.bfloat16
    )
    mixer_terms = jnp.dot(
        grouped,
        lax.all_gather(pool_output, "fs", axis=1, tiled=True),
        preferred_element_type=jnp.float32,
    )
    mixer_out = lax.psum_scatter(
        mixer_terms.astype(jnp.bfloat16), "tp", scatter_dimension=1, tiled=True
    ).astype(jnp.float32)
    middle = (tokens.astype(jnp.float32) + mixer_out).astype(jnp.bfloat16)
    middle_rows = lax.all_gather(middle, "tp", axis=1, tiled=True)
    second_normed = rms(middle_rows, ffn_gain).astype(jnp.bfloat16)
    gate = add_rows(second_normed, lax.all_gather(gate_weight, "fs", axis=0, tiled=True))
    upward = add_rows(second_normed, lax.all_gather(up_weight, "fs", axis=0, tiled=True))
    hidden = (jax.nn.silu(gate) * upward).astype(jnp.bfloat16)
    ffn_terms = jnp.dot(
        hidden,
        lax.all_gather(down_weight, "fs", axis=1, tiled=True),
        preferred_element_type=jnp.float32,
    )
    ffn_out = lax.psum_scatter(
        ffn_terms.astype(jnp.bfloat16), "tp", scatter_dimension=1, tiled=True
    ).astype(jnp.float32)
    closing = middle.astype(jnp.float32) + ffn_out
    squares = lax.psum(jnp.sum(closing * closing, axis=1, keepdims=True), "tp")
    scaled = closing * lax.rsqrt(squares / D + EPS) * final_gain
    return scaled.astype(jnp.bfloat16)


def solution(mesh):
    placed = (
        P("fs", "tp"),
        P(),
        P("fs", "tp"),
        P("tp", None, None),
        P("tp"),
        P("tp", "fs"),
        P(),
        P("fs", "tp"),
        P("fs", "tp"),
        P("tp", "fs"),
        P("tp"),
    )
    return jax.shard_map(
        local, mesh=mesh, in_specs=placed, out_specs=P("fs", "tp"), check_vma=False
    )
```

profile of v0, /device:TPU:0, one launch (start us, length us, event | category | flops | bytes accessed | tf_op | source)
XLA Modules:
  0.0 684.9 jit_solution(15526173825975011963)
XLA Ops:
  6.5 0.7 all-gather.8.cloned.1.call-update
  7.3 0.7 all-gather.10.cloned.1.call-update
  8.1 0.7 all-gather.12.cloned.1.call-update
  9.0 12.4 %all-gather.8.cloned.1.call-done = bf16[384,2048]{1,0:T(8,128)(2,1)} async-done(((bf16[384,1024]{1,0:T(8,128)(2,1)}), bf16[384,2048]{1,0:T(8,128)(2,1)}) %all-gather.8.cloned.1.call-update) | async-done | bytes 1572880 | tf_op jit(solution)/shard_map/all_gather | solution.py:35
  21.4 1.8 fusion.1
  23.2 62.6 %all-gather.10.cloned.1.call-done = bf16[2048,512]{1,0:T(8,128)(2,1)} async-done(((bf16[128,512]{1,0:T(8,128)(2,1)}), bf16[2048,512]{1,0:T(8,128)(2,1)}) %all-gather.10.cloned.1.call-update) | async-done | bytes 2097168 | tf_op jit(solution)/shard_map/all_gather | solution.py:38
  85.8 3.1 fusion.14
  89.8 60.4 %all-gather.12.cloned.1.call-done = bf16[512,2048]{1,0:T(8,128)(2,1)} async-done(((bf16[512,128]{1,0:T(8,128)(2,1)}), bf16[512,2048]{1,0:T(8,128)(2,1)}) %all-gather.12.cloned.1.call-update) | async-done | bytes 2097168 | tf_op jit(solution)/shard_map/all_gather | solution.py:64
  150.3 3.8 convolution_convert_fusion.1
  154.1 7.2 %reduce-scatter.3.cloned.1.call-done = bf16[384,1024]{1,0:T(8,128)(2,1)} async-done(((bf16[384,2048]{1,0:T(8,128)(2,1)}), bf16[384,1024]{1,0:T(8,128)(2,1)}) %reduce-scatter.3.cloned.1.call-update) | async-done | bytes 786448 | tf_op jit(solution)/shard_map/reduce_scatter | solution.py:67
  161.4 2.3 add_convert_fusion
  164.3 0.7 all-gather.18.cloned.1.call-update
  165.1 0.7 all-gather.20.cloned.1.call-update
  166.0 8.9 %all-gather.14.cloned.1.call-done = bf16[384,2048]{1,0:T(8,128)(2,1)} async-done(((bf16[384,1024]{1,0:T(8,128)(2,1)}), bf16[384,2048]{1,0:T(8,128)(2,1)}) %all-gather.14.cloned.1.call-update) | async-done | bytes 1572880 | tf_op jit(solution)/shard_map/all_gather | solution.py:71
  174.9 1.8 fusion.4
  176.7 143.4 %all-gather.16.cloned.1.call-done = bf16[2048,2816]{1,0:T(8,128)(2,1)} async-done(((bf16[128,2816]{1,0:T(8,128)(2,1)}), bf16[2048,2816]{1,0:T(8,128)(2,1)}) %all-gather.16.cloned.1.call-update) | async-done | bytes 11534352 | tf_op jit(solution)/shard_map/all_gather | solution.py:73
  320.2 11.5 %fusion.20 = f32[384,2816]{1,0:T(8,128)} fusion(bf16[2048,2816]{1,0:T(8,128)(2,1)} %all-gather.16.cloned.1.call-done, bf16[384,2048]{1,0:T(8,128)(2,1)} %all-gather.14.cloned.1.call-done, f32[2048]{0:T(1024)S(1)} %copy-done.6, f32[384]{0:T(512)S(1)} %add_rsqrt_fusion), kind=kOutput, calls=%fused_computation.28 | convolution fusion | flops 4432330752 | bytes 17442304 | tf_op jit(solution)/shard_map/dot_general | solution.py:19
  331.7 130.8 %all-gather.18.cloned.1.call-done = bf16[2048,2816]{1,0:T(8,128)(2,1)} async-done(((bf16[128,2816]{1,0:T(8,128)(2,1)}), bf16[2048,2816]{1,0:T(8,128)(2,1)}) %all-gather.18.cloned.1.call-update) | async-done | bytes 11534352 | tf_op jit(solution)/shard_map/all_gather | solution.py:74
  462.5 183.0 %all-gather.20.cloned.1.call-done = bf16[2816,2048]{1,0:T(8,128)(2,1)} async-done(((bf16[2816,128]{1,0:T(8,128)(2,1)}), bf16[2816,2048]{1,0:T(8,128)(2,1)}) %all-gather.20.cloned.1.call-update) | async-done | bytes 11534352 | tf_op jit(solution)/shard_map/all_gather | solution.py:78
  645.5 19.3 %convolution_convert_fusion = bf16[384,2048]{1,0:T(8,128)(2,1)} fusion(bf16[2816,2048]{1,0:T(8,128)(2,1)} %all-gather.20.cloned.1.call-done, bf16[2048,2816]{1,0:T(8,128)(2,1)} %all-gather.18.cloned.1.call-done, f32[384,2816]{1,0:T(8,128)} %fusion.20, bf16[384,2048]{1,0:T(8,128)(2,1)S(1)} %copy-done.3, f32[2048]{0:T(1024)S(1)} %copy-done.6, ...), kind=kOutput, calls=%fused_computation.12 | convolution fusion | flops 8868790272 | bytes 30549504 | tf_op jit(solution)/shard_map/dot_general | solution.py:76
  664.8 7.3 %reduce-scatter.5.cloned.1.call-done = bf16[384,1024]{1,0:T(8,128)(2,1)} async-done(((bf16[384,2048]{1,0:T(8,128)(2,1)}), bf16[384,1024]{1,0:T(8,128)(2,1)}) %reduce-scatter.5.cloned.1.call-update) | async-done | bytes 786448 | tf_op jit(solution)/shard_map/reduce_scatter | solution.py:81
  672.1 1.5 multiply_reduce_fusion
  673.6 2.5 psum.7
  676.1 2.3 multiply_convert_fusion
  (40 shorter events, 2.2 us)
Async XLA Ops:
  6.5 82.8 %copy-start = (bf16[4,128,128]{2,1,0:T(8,128)(2,1)S(1)}, bf16[4,128,128]{2,1,0:T(8,128)(2,1)}, u32[]{:S(2)}) copy-start(bf16[4,128,128]{2,1,0:T(8,128)(2,1)} %param.14) | copy-start | bytes 393220
  6.5 14.9 %all-gather.8.cloned.1.call-start = ((), (), s32[]{:S(2)}) async-start(), calls=%async_computation.2 | async-start | bytes 2359296 | tf_op jit(solution)/shard_map/all_gather | solution.py:35
  7.3 78.5 %all-gather.10.cloned.1.call-start = ((), (), s32[]{:S(2)}) async-start(), calls=%async_computation.3 | async-start | bytes 2228224 | tf_op jit(solution)/shard_map/all_gather | solution.py:38
  8.0 142.3 %all-gather.12.cloned.1.call-start = ((), (), s32[]{:S(2)}) async-start(), calls=%async_computation.4 | async-start | bytes 2228224 | tf_op jit(solution)/shard_map/all_gather | solution.py:64
  8.7 152.6 %reduce-scatter.3.cloned.1.call-start = ((), (), s32[]{:S(2)}) async-start(), calls=%async_computation.5 | async-start | bytes 2359296 | tf_op jit(solution)/shard_map/reduce_scatter | solution.py:67
  88.9 0.8 copy-start.5
  89.7 71.7 %copy-start.2 = (bf16[384,1024]{1,0:T(8,128)(2,1)S(1)}, bf16[384,1024]{1,0:T(8,128)(2,1)}, u32[]{:S(2)}) copy-start(bf16[384,1024]{1,0:T(8,128)(2,1)} %param.11) | copy-start | bytes 2359300
  154.1 166.1 %copy-start.6 = (f32[2048]{0:T(1024)S(1)}, f32[2048]{0:T(1024)}, u32[]{:S(2)}) copy-start(f32[2048]{0:T(1024)} %param.17) | copy-start | bytes 24580
  154.1 20.8 %all-gather.14.cloned.1.call-start = ((), (), s32[]{:S(2)}) async-start(), calls=%async_computation.6 | async-start | bytes 2359296 | tf_op jit(solution)/shard_map/all_gather | solution.py:71
  163.7 156.5 %all-gather.16.cloned.1.call-start = ((), (), s32[]{:S(2)}) async-start(), calls=%async_computation.7 | async-start | bytes 12255232 | tf_op jit(solution)/shard_map/all_gather | solution.py:73
  164.3 298.3 %all-gather.18.cloned.1.call-start = ((), (), s32[]{:S(2)}) async-start(), calls=%async_computation.8 | async-start | bytes 12255232 | tf_op jit(solution)/shard_map/all_gather | solution.py:74
  165.0 480.5 %all-gather.20.cloned.1.call-start = ((), (), s32[]{:S(2)}) async-start(), calls=%async_computation.9 | async-start | bytes 12255232 | tf_op jit(solution)/shard_map/all_gather | solution.py:78
  165.8 506.3 %reduce-scatter.5.cloned.1.call-start = ((), (), s32[]{:S(2)}) async-start(), calls=%async_computation.10 | async-start | bytes 2359296 | tf_op jit(solution)/shard_map/reduce_scatter | solution.py:81
  176.7 468.8 %copy-start.3 = (bf16[384,2048]{1,0:T(8,128)(2,1)S(1)}, bf16[384,2048]{1,0:T(8,128)(2,1)}, u32[]{:S(2)}) copy-start(bf16[384,2048]{1,0:T(8,128)(2,1)} %all-gather.14.cloned.1.call-done) | copy-start | bytes 4718596
  331.7 340.4 %copy-start.1 = (bf16[384,1024]{1,0:T(8,128)(2,1)S(1)}, bf16[384,1024]{1,0:T(8,128)(2,1)}, u32[]{:S(2)}) copy-start(bf16[384,1024]{1,0:T(8,128)(2,1)} %add_convert_fusion) | copy-start | bytes 2359300
  664.8 11.3 %copy-start.4 = (f32[1024]{0:T(1024)S(1)}, f32[1024]{0:T(1024)}, u32[]{:S(2)}) copy-start(f32[1024]{0:T(1024)} %param.21) | copy-start | bytes 12292
Sparse Core Ops, SparseCore 0:
  8.9 12.5 all-gather.7
  24.2 61.5 all-gather.9
  88.5 61.7 all-gather.11
  154.2 7.1 reduce-scatter.2
  163.8 11.0 all-gather.13
  177.5 142.5 all-gather.15
  322.9 139.5 all-gather.17
  465.3 180.2 all-gather.19
  664.9 7.1 reduce-scatter.4
where the time goes:
time: 685 us
  waiting for transfers between devices  620 us (91%)
  matrix products  38.3 us (6%)
  between operations  13.3 us (2%)
  other arithmetic  10 us (1%)
    all_gather x1, waiting for transfers between devices, local(): lax.all_gather(down_weight, 'fs', axis=1, tiled=True)  183 us
    all_gather x1, waiting for transfers between devices, local(): lax.all_gather(gate_weight, 'fs', axis=0, tiled=True)  143 us
    all_gather x1, waiting for transfers between devices, local(): lax.all_gather(up_weight, 'fs', axis=0, tiled=True)  131 us
    all_gather x1, waiting for transfers between devices, local(): lax.all_gather(pool_input, 'fs', axis=0, tiled=True)  62.6 us
    all_gather x1, waiting for transfers between devices, local(): lax.all_gather(pool_output, 'fs', axis=1, tiled=True)  60.4 us
    dot_general x1, matrix products, local(): jnp.dot(hidden, lax.all_gather(down_weight, 'fs', axis=1, tiled=True), pr...  19.3 us
    dot_general x2, matrix products, add_rows(): return jnp.dot(left, piece, preferred_element_type=jnp.float32)  14.6 us
  transfers between devices with their start and end apart: 9, of which 9 were waited for; matrix products, arithmetic and copies ran while one was open for 3% of the time, Pallas kernels for 0%

commit v1 on v0

--- a/solution.py
+++ b/solution.py
@@ -75,7 +75,9 @@
     hidden = (jax.nn.silu(gate) * upward).astype(jnp.bfloat16)
     ffn_terms = jnp.dot(
         hidden,
-        lax.all_gather(down_weight, "fs", axis=1, tiled=True),
+        jnp.concatenate(
+            lax.all_to_all(jnp.stack([down_weight] * lax.axis_size("fs")), "fs", 0, 0), axis=1
+        ),
         preferred_element_type=jnp.float32,
     )
     ffn_out = lax.psum_scatter(

time: 685 us -> 723 us (1.055)
  waiting for transfers between devices: 620 us -> 643 us
    all_gather x1, waiting for transfers between devices: 143 us -> 348 us  [local(): lax.all_gather(gate_weight, 'fs', axis=0, tiled=True)]
    all_gather x1 -> x0, waiting for transfers between devices: 183 us -> none  [local(): lax.all_gather(down_weight, 'fs', axis=1, tiled=True)]
    all_gather x1, waiting for transfers between devices: 131 us -> 142 us  [local(): lax.all_gather(up_weight, 'fs', axis=0, tiled=True)]
    all_gather x1, waiting for transfers between devices: 8.92 us -> 0.02 us  [local(): middle_rows = lax.all_gather(middle, 'tp', axis=1, tiled=True)]
  transfers between devices with their start and end apart: 9 -> 9, of which waited for: 9 -> 7; matrix products, arithmetic and copies ran while one was open for 3% -> 3% of each run, Pallas kernels for 0% -> 0%
where the time goes in v1:
time: 723 us; the launch traced here: 722 us
  waiting for transfers between devices  643 us (89%)
  matrix products  40.5 us (6%)
  between operations  13.6 us (2%)
  other arithmetic  10 us (1%)
  starting transfers between devices  7.53 us (1%)
    all_gather x1, waiting for transfers between devices, local(): lax.all_gather(gate_weight, 'fs', axis=0, tiled=True)  348 us
    all_gather x1, waiting for transfers between devices, local(): lax.all_gather(up_weight, 'fs', axis=0, tiled=True)  142 us
    all_gather x1, waiting for transfers between devices, local(): lax.all_gather(pool_input, 'fs', axis=0, tiled=True)  62.6 us
    all_gather x1, waiting for transfers between devices, local(): lax.all_gather(pool_output, 'fs', axis=1, tiled=True)  60.4 us
    dot_general x1, matrix products, local(): jnp.dot(hidden, jnp.concatenate(lax.all_to_all(jnp.stack([down_weight] *...  21.5 us
    dot_general x2, matrix products, add_rows(): return jnp.dot(left, piece, preferred_element_type=jnp.float32)  14.5 us
  transfers between devices with their start and end apart: 9, of which 7 were waited for; matrix products, arithmetic and copies ran while one was open for 3% of the time, Pallas kernels for 0%

profile of v1, /device:TPU:0, one launch (start us, length us, event | category | flops | bytes accessed | tf_op | source)
XLA Modules:
  0.0 722.5 jit_solution(14741517472112223155)
XLA Ops:
  6.5 0.7 all-gather.7.cloned.1.call-update
  7.3 0.7 all-gather.9.cloned.1.call-update
  8.1 0.7 all-gather.11.cloned.1.call-update
  9.0 12.4 %all-gather.7.cloned.1.call-done = bf16[384,2048]{1,0:T(8,128)(2,1)} async-done(((bf16[384,1024]{1,0:T(8,128)(2,1)}), bf16[384,2048]{1,0:T(8,128)(2,1)}) %all-gather.7.cloned.1.call-update) | async-done | bytes 1572880 | tf_op jit(solution)/shard_map/all_gather | solution.py:35
  21.4 1.8 fusion.1
  23.2 62.6 %all-gather.9.cloned.1.call-done = bf16[2048,512]{1,0:T(8,128)(2,1)} async-done(((bf16[128,512]{1,0:T(8,128)(2,1)}), bf16[2048,512]{1,0:T(8,128)(2,1)}) %all-gather.9.cloned.1.call-update) | async-done | bytes 2097168 | tf_op jit(solution)/shard_map/all_gather | solution.py:38
  85.8 3.1 fusion.14
  89.8 60.4 %all-gather.11.cloned.1.call-done = bf16[512,2048]{1,0:T(8,128)(2,1)} async-done(((bf16[512,128]{1,0:T(8,128)(2,1)}), bf16[512,2048]{1,0:T(8,128)(2,1)}) %all-gather.11.cloned.1.call-update) | async-done | bytes 2097168 | tf_op jit(solution)/shard_map/all_gather | solution.py:64
  150.3 3.8 convolution_convert_fusion.1
  154.1 7.2 %reduce-scatter.3.cloned.1.call-done = bf16[384,1024]{1,0:T(8,128)(2,1)} async-done(((bf16[384,2048]{1,0:T(8,128)(2,1)}), bf16[384,1024]{1,0:T(8,128)(2,1)}) %reduce-scatter.3.cloned.1.call-update) | async-done | bytes 786448 | tf_op jit(solution)/shard_map/reduce_scatter | solution.py:67
  161.3 2.3 add_convert_fusion
  163.7 0.5 all-gather.15.cloned.1.call-update
  164.6 5.3 stack.2
  169.9 7.1 all-to-all-start
  177.0 0.7 all-gather.17.cloned.1.call-update
  177.9 1.8 fusion.4
  179.7 347.8 %all-gather.15.cloned.1.call-done = bf16[2048,2816]{1,0:T(8,128)(2,1)} async-done(((bf16[128,2816]{1,0:T(8,128)(2,1)}), bf16[2048,2816]{1,0:T(8,128)(2,1)}) %all-gather.15.cloned.1.call-update) | async-done | bytes 11534352 | tf_op jit(solution)/shard_map/all_gather | solution.py:73
  527.5 11.4 %fusion.20 = f32[384,2816]{1,0:T(8,128)} fusion(bf16[2048,2816]{1,0:T(8,128)(2,1)} %all-gather.15.cloned.1.call-done, bf16[384,2048]{1,0:T(8,128)(2,1)} %all-gather.13.cloned.1.call-done, f32[2048]{0:T(1024)S(1)} %copy-done.8, f32[384]{0:T(512)S(1)} %add_rsqrt_fusion), kind=kOutput, calls=%fused_computation.28 | convolution fusion | flops 4432330752 | bytes 17442304 | tf_op jit(solution)/shard_map/dot_general | solution.py:19
  539.0 141.5 %all-gather.17.cloned.1.call-done = bf16[2048,2816]{1,0:T(8,128)(2,1)} async-done(((bf16[128,2816]{1,0:T(8,128)(2,1)}), bf16[2048,2816]{1,0:T(8,128)(2,1)}) %all-gather.17.cloned.1.call-update) | async-done | bytes 11534352 | tf_op jit(solution)/shard_map/all_gather | solution.py:74
  680.5 21.5 %convolution_convert_fusion = bf16[384,2048]{1,0:T(8,128)(2,1)} fusion(bf16[2816,2048]{0,1:T(8,128)(2,1)} %bitcast.7, bf16[2048,2816]{1,0:T(8,128)(2,1)} %all-gather.17.cloned.1.call-done, f32[384,2816]{1,0:T(8,128)} %fusion.20, bf16[384,2048]{1,0:T(8,128)(2,1)S(1)} %copy-done.4, f32[2048]{0:T(1024)S(1)} %copy-done.8, f32[384]{0:T(512)S(1)} %add_rsqrt_fusion), kind=kOutput, calls=%fused_computation.12 | convolution fusion | flops 8868790272 | bytes 30549504 | tf_op jit(solution)/shard_map/dot_general | solution.py:76
  702.0 7.3 %reduce-scatter.5.cloned.1.call-done = bf16[384,1024]{1,0:T(8,128)(2,1)} async-done(((bf16[384,2048]{1,0:T(8,128)(2,1)}), bf16[384,1024]{1,0:T(8,128)(2,1)}) %reduce-scatter.5.cloned.1.call-update) | async-done | bytes 786448 | tf_op jit(solution)/shard_map/reduce_scatter | solution.py:83
  709.3 1.5 multiply_reduce_fusion
  710.8 2.5 psum.7
  713.3 2.3 multiply_convert_fusion
  (45 shorter events, 1.9 us)
Async XLA Ops:
  6.5 82.8 %copy-start = (bf16[4,128,128]{2,1,0:T(8,128)(2,1)S(1)}, bf16[4,128,128]{2,1,0:T(8,128)(2,1)}, u32[]{:S(2)}) copy-start(bf16[4,128,128]{2,1,0:T(8,128)(2,1)} %param.14) | copy-start | bytes 393220
  6.5 14.9 %all-gather.7.cloned.1.call-start = ((), (), s32[]{:S(2)}) async-start(), calls=%async_computation.3 | async-start | bytes 2359296 | tf_op jit(solution)/shard_map/all_gather | solution.py:35
  7.3 78.5 %all-gather.9.cloned.1.call-start = ((), (), s32[]{:S(2)}) async-start(), calls=%async_computation.4 | async-start | bytes 2228224 | tf_op jit(solution)/shard_map/all_gather | solution.py:38
  8.0 142.3 %all-gather.11.cloned.1.call-start = ((), (), s32[]{:S(2)}) async-start(), calls=%async_computation.5 | async-start | bytes 2228224 | tf_op jit(solution)/shard_map/all_gather | solution.py:64
  8.7 152.6 %reduce-scatter.3.cloned.1.call-start = ((), (), s32[]{:S(2)}) async-start(), calls=%async_computation.6 | async-start | bytes 2359296 | tf_op jit(solution)/shard_map/reduce_scatter | solution.py:67
  88.9 0.8 copy-start.7
  89.7 71.7 %copy-start.3 = (bf16[384,1024]{1,0:T(8,128)(2,1)S(1)}, bf16[384,1024]{1,0:T(8,128)(2,1)}, u32[]{:S(2)}) copy-start(bf16[384,1024]{1,0:T(8,128)(2,1)} %param.11) | copy-start | bytes 2359300
  154.0 10.2 %copy-start.5 = (bf16[2816,128]{1,0:T(8,128)(2,1)S(1)}, bf16[2816,128]{1,0:T(8,128)(2,1)}, u32[]{:S(2)}) copy-start(bf16[2816,128]{1,0:T(8,128)(2,1)} %param.20) | copy-start | bytes 2162692
  154.1 23.9 %all-gather.13.cloned.1.call-start = ((), (), s32[]{:S(2)}) async-start(), calls=%async_computation.7 | async-start | bytes 2359296 | tf_op jit(solution)/shard_map/all_gather | solution.py:71
  163.7 363.8 %all-gather.15.cloned.1.call-start = ((), (), s32[]{:S(2)}) async-start(), calls=%async_computation.8 | async-start | bytes 12255232 | tf_op jit(solution)/shard_map/all_gather | solution.py:73
  169.9 357.7 %copy-start.8 = (f32[2048]{0:T(1024)S(1)}, f32[2048]{0:T(1024)}, u32[]{:S(2)}) copy-start(f32[2048]{0:T(1024)} %param.17) | copy-start | bytes 24580
  169.9 369.1 %all-to-all-start = ((bf16[16,2816,128]{1,2,0:T(8,128)(2,1)}), bf16[16,2816,128]{1,2,0:T(8,128)(2,1)}, u32[]{:S(2)}, u32[]{:S(2)}) async-start(bf16[16,2816,128]{1,2,0:T(8,128)(2,1)} %stack.2), calls=%async_computation.1 | async-start | bytes 23068672 | tf_op jit(solution)/shard_map/all_to_all | solution.py:79
  176.9 503.6 %all-gather.17.cloned.1.call-start = ((), (), s32[]{:S(2)}) async-start(), calls=%async_computation.9 | async-start | bytes 12255232 | tf_op jit(solution)/shard_map/all_gather | solution.py:74
  177.7 531.6 %reduce-scatter.5.cloned.1.call-start = ((), (), s32[]{:S(2)}) async-start(), calls=%async_computation.10 | async-start | bytes 2359296 | tf_op jit(solution)/shard_map/reduce_scatter | solution.py:83
  179.7 500.8 %copy-start.4 = (bf16[384,2048]{1,0:T(8,128)(2,1)S(1)}, bf16[384,2048]{1,0:T(8,128)(2,1)}, u32[]{:S(2)}) copy-start(bf16[384,2048]{1,0:T(8,128)(2,1)} %all-gather.13.cloned.1.call-done) | copy-start | bytes 4718596
  680.5 28.8 %copy-start.2 = (bf16[384,1024]{1,0:T(8,128)(2,1)S(1)}, bf16[384,1024]{1,0:T(8,128)(2,1)}, u32[]{:S(2)}) copy-start(bf16[384,1024]{1,0:T(8,128)(2,1)} %add_convert_fusion) | copy-start | bytes 2359300
  680.5 35.1 %copy-start.1 = (bf16[4,128,128]{2,1,0:T(8,128)(2,1)S(1)}, bf16[4,128,128]{2,1,0:T(8,128)(2,1)}, u32[]{:S(2)}) copy-start(bf16[4,128,128]{2,1,0:T(8,128)(2,1)} %param.14) | copy-start | bytes 393220
  702.0 11.3 %copy-start.6 = (f32[1024]{0:T(1024)S(1)}, f32[1024]{0:T(1024)}, u32[]{:S(2)}) copy-start(f32[1024]{0:T(1024)} %param.21) | copy-start | bytes 12292
Sparse Core Ops, SparseCore 0:
  8.9 12.5 all-gather.6
  24.2 61.5 all-gather.8
  88.5 61.7 all-gather.10
  154.2 7.1 reduce-scatter.2
  163.8 11.0 all-gather.12
  177.5 349.9 all-gather.14
  530.3 150.1 all-gather.16
  702.2 7.1 reduce-scatter.4
